TPU v7x, 32 devices: a whole 2x2x4 slice. The times are simulated.
32 devices in a mesh: kv: 4 (over y, x), tp: 8 (over z, core).
Axes of the slice: x: 2, y: 2, z: 4, core: 2. Of those that a mesh axis runs over, the one named last changes fastest.
Arguments:
- tokens: bfloat16 [256, 4096], P(None, ('kv', 'tp')), may hold values from -10 to 10
- past_state: float32 [256, 32, 64, 128], P('kv', 'tp'), may hold values from -6 to 6
- first_gain: float32 [4096], P('kv'), may hold values from 0.1 to 1.9
- first_gate: bfloat16 [4096, 11264], P('kv', 'tp'), may hold values from -0.09375 to 0.09375
- first_up: bfloat16 [4096, 11264], P('kv', 'tp'), may hold values from -0.09375 to 0.09375
- first_down: bfloat16 [11264, 4096], P('tp', 'kv'), may hold values from -0.078125 to 0.078125
- mix_gain: float32 [4096], P('kv'), may hold values from 0.1 to 1.9
- query_weight: bfloat16 [4096, 2048], P('kv', 'tp'), may hold values from -0.09375 to 0.09375
- key_weight: bfloat16 [4096, 2048], P('kv', 'tp'), may hold values from -0.09375 to 0.09375
- value_weight: bfloat16 [4096, 4096], P('kv', 'tp'), may hold values from -0.09375 to 0.09375
- output_gate_weight: bfloat16 [4096, 4096], P('kv', 'tp'), may hold values from -0.09375 to 0.09375
- head_gain: float32 [4096], P('tp'), may hold values from 0.1 to 1.9
- out_weight: bfloat16 [4096, 4096], P('tp', 'kv'), may hold values from -0.125 to 0.125
- second_gain: float32 [4096], P('kv'), may hold values from 0.1 to 1.9
- second_gate: bfloat16 [4096, 11264], P('kv', 'tp'), may hold values from -0.09375 to 0.09375
- second_up: bfloat16 [4096, 11264], P('kv', 'tp'), may hold values from -0.09375 to 0.09375
- second_down: bfloat16 [11264, 4096], P('tp', 'kv'), may hold values from -0.078125 to 0.078125
Outputs:
- mixed: bfloat16 [256, 4096], P(None, ('kv', 'tp'))
- new_state: float32 [256, 32, 64, 128], P('kv', 'tp')
All inputs are finite; a program needn't handle non-finite values.
Results may differ from a plain program's by a relative error of at most 0.033.
Values may be sent and summed in bfloat16 or wider, within the bound.
A program may use at most 128 MiB of HBM per device.

v0:
```python
import jax
import jax.numpy as jnp
from jax import lax
from jax.sharding import PartitionSpec as P

D = 4096
HEADS = 32
HEAD_K = 64
HEAD_V = 128
POS = 16384
EPS_RMS = 1e-06
EPS_GROUP = 1e-05
ROPE_BASE = 10000.0


def rotate(vectors):
    half_width = vectors.shape[-1] // 2
    frequency = ROPE_BASE ** (-jnp.arange(half_width, dtype=jnp.float32) / half_width)
    angles = POS * frequency
    cosine = jnp.cos(angles)
    sine_part = jnp.sin(angles)
    lower = vectors[..., :half_width]
    upper = vectors[..., half_width:]
    return jnp.concatenate(
        [lower * cosine - upper * sine_part, lower * sine_part + upper * cosine], axis=-1
    )


def activate(gate_sum, up_sum, summed):
    inverse_rms = lax.rsqrt(summed / D + EPS_RMS)[:, None]
    return (jax.nn.silu(gate_sum * inverse_rms) * (up_sum * inverse_rms)).astype(jnp.bfloat16)


def channel_mix(widened, gain, w_gate, w_up, w_down):
    widened_f = widened.astype(jnp.float32)
    scaled = (widened_f * gain).astype(jnp.bfloat16)
    squares = jnp.sum(widened_f * widened_f, axis=1)
    gate_part = jnp.dot(scaled, w_gate, preferred_element_type=jnp.float32)
    up_part = jnp.dot(scaled, w_up, preferred_element_type=jnp.float32)
    gate_sum, up_sum, summed = (
        lax.psum(gate_part.astype(jnp.bfloat16), "kv").astype(jnp.float32),
        lax.psum(up_part.astype(jnp.bfloat16), "kv").astype(jnp.float32),
        lax.psum(squares.astype(jnp.bfloat16), "kv").astype(jnp.float32),
    )
    return 0.5 * jnp.dot(
        activate(gate_sum, up_sum, summed), w_down, preferred_element_type=jnp.float32
    )


def token_mix(
    widened,
    past_state,
    gain,
    query_weight,
    key_weight,
    value_weight,
    output_gate_weight,
    head_gain,
    out_weight,
):
    widened_f = widened.astype(jnp.float32)
    scaled = (widened_f * gain).astype(jnp.bfloat16)
    squares = jnp.sum(widened_f * widened_f, axis=1)
    query_part = jnp.dot(scaled, query_weight, preferred_element_type=jnp.float32)
    key_part = jnp.dot(scaled, key_weight, preferred_element_type=jnp.float32)
    value_part = jnp.dot(scaled, value_weight, preferred_element_type=jnp.float32)
    gate_part = jnp.dot(scaled, output_gate_weight, preferred_element_type=jnp.float32)
    queries, keys_now, values_now, gate_now, summed = (
        lax.psum_scatter(
            query_part.astype(jnp.bfloat16), "kv", scatter_dimension=0, tiled=True
        ).astype(jnp.float32),
        lax.psum_scatter(
            key_part.astype(jnp.bfloat16), "kv", scatter_dimension=0, tiled=True
        ).astype(jnp.float32),
        lax.psum_scatter(
            value_part.astype(jnp.bfloat16), "kv", scatter_dimension=0, tiled=True
        ).astype(jnp.float32),
        lax.psum_scatter(
            gate_part.astype(jnp.bfloat16), "kv", scatter_dimension=0, tiled=True
        ).astype(jnp.float32),
        lax.psum_scatter(
            squares.astype(jnp.bfloat16), "kv", scatter_dimension=0, tiled=True
        ).astype(jnp.float32),
    )
    inverse_rms = lax.rsqrt(summed / D + EPS_RMS)[:, None]
    row_count = past_state.shape[0]
    local_heads = past_state.shape[1]
    queries = rotate((queries * inverse_rms).reshape(row_count, local_heads, HEAD_K)) * HEAD_K ** (
        -0.5
    )
    keys_now = rotate((keys_now * inverse_rms).reshape(row_count, local_heads, HEAD_K))
    values_now = (values_now * inverse_rms).reshape(row_count, local_heads, HEAD_V)
    gate_now = gate_now * inverse_rms
    head_level = (lax.axis_index("tp") * local_heads + jnp.arange(local_heads)).astype(jnp.float32)
    retained = 1.0 - jnp.exp2(-5.0 - 16.0 * head_level / (HEADS - 1))
    new_state = (
        retained[None, :, None, None] * past_state
        + keys_now[:, :, :, None] * values_now[:, :, None, :]
    )
    retrieved = jnp.einsum("bhk,bhkv->bhv", queries, new_state, precision=lax.Precision.HIGHEST)
    head_mean = jnp.mean(retrieved, axis=-1, keepdims=True)
    variance = jnp.mean(jnp.square(retrieved - head_mean), axis=-1, keepdims=True)
    normed = ((retrieved - head_mean) * lax.rsqrt(variance + EPS_GROUP)).reshape(
        row_count, local_heads * HEAD_V
    )
    mixed_heads = (jax.nn.silu(gate_now) * (normed * head_gain)).astype(jnp.bfloat16)
    projected = jnp.dot(
        lax.all_gather(mixed_heads, "kv", axis=0, tiled=True),
        out_weight,
        preferred_element_type=jnp.float32,
    )
    return (projected, new_state)


def shards(
    tokens,
    past_state,
    first_gain,
    first_gate,
    first_up,
    first_down,
    mix_gain,
    query_weight,
    key_weight,
    value_weight,
    output_gate_weight,
    head_gain,
    out_weight,
    second_gain,
    second_gate,
    second_up,
    second_down,
):

    def first_section(widened):
        return (channel_mix(widened, first_gain, first_gate, first_up, first_down), None)

    def middle_section(widened):
        return token_mix(
            widened,
            past_state,
            mix_gain,
            query_weight,
            key_weight,
            value_weight,
            output_gate_weight,
            head_gain,
            out_weight,
        )

    def last_section(widened):
        return (channel_mix(widened, second_gain, second_gate, second_up, second_down), None)

    sections = [first_section, middle_section, last_section]
    own_columns = tokens
    widened = lax.all_gather(tokens, "tp", axis=1, tiled=True)
    state_out = past_state
    for section_index in range(3):
        branch_out, produced = sections[section_index](widened)
        if produced is not None:
            state_out = produced
        own_piece = lax.psum_scatter(
            branch_out.astype(jnp.bfloat16), "tp", scatter_dimension=1, tiled=True
        ).astype(jnp.float32)
        own_columns = (own_columns.astype(jnp.float32) + own_piece).astype(jnp.bfloat16)
        if section_index < 2:
            widened = lax.all_gather(own_columns, "tp", axis=1, tiled=True)
    return (own_columns, state_out)


def solution(mesh):
    in_specs = (
        P(None, ("kv", "tp")),
        P("kv", "tp", None, None),
        P("kv"),
        P("kv", "tp"),
        P("kv", "tp"),
        P("tp", "kv"),
        P("kv"),
        P("kv", "tp"),
        P("kv", "tp"),
        P("kv", "tp"),
        P("kv", "tp"),
        P("tp"),
        P("tp", "kv"),
        P("kv"),
        P("kv", "tp"),
        P("kv", "tp"),
        P("tp", "kv"),
    )
    out_specs = (P(None, ("kv", "tp")), P("kv", "tp", None, None))
    return jax.shard_map(shards, mesh=mesh, in_specs=in_specs, out_specs=out_specs, check_vma=False)
```

profile of v0, /device:TPU:0, one launch (start us, length us, event | category | flops | bytes accessed | tf_op | source)
XLA Modules:
  0.0 409.7 jit_solution(10858656113238108868)
XLA Ops:
  7.2 15.8 %all_gather.12 = bf16[256,1024]{1,0:T(8,128)(2,1)S(1)} all-gather(bf16[256,128]{1,0:T(8,128)(2,1)} %param.17), channel_id=1, replica_groups=mesh['kv'=4,'tp'=8] {'tp'}, dimensions={1}, use_global_device_ids=true | all-gather | bytes 589824 | tf_op jit(solution)/shard_map/all_gather | solution.py:156
  23.0 2.5 convolution_convert_fusion.2
  25.6 1.9 convolution_convert_fusion.3
  27.7 10.1 %psum.43 = bf16[256]{0:T(256)(128)(2,1)S(1)} all-reduce(bf16[256]{0:T(256)(128)(2,1)S(1)} %fusion.3), channel_id=1, replica_groups=mesh['kv'=4,'tp'=8] {'kv'}, use_global_device_ids=true, to_apply=%region_2.0 | all-reduce | flops 256 | bytes 1024 | tf_op jit(solution)/shard_map/psum | solution.py:43
  37.8 48.4 %all-reduce.8.cloned.1.call-done = (bf16[256,1408]{1,0:T(8,128)(2,1)}, bf16[256,1408]{1,0:T(8,128)(2,1)}) async-done(((bf16[256,1408]{1,0:T(8,128)(2,1)}, bf16[256,1408]{1,0:T(8,128)(2,1)}), (bf16[256,1408]{1,0:T(8,128)(2,1)}, bf16[256,1408]{1,0:T(8,128)(2,1)})) %all-reduce.8.cloned.1.call-update) | async-done | bytes 1441808 | tf_op jit(solution)/shard_map/psum | solution.py:42
  86.2 3.5 fusion
  89.7 1.0 copy.24
  90.8 31.2 %reduce-scatter.22.cloned.1.call-done = bf16[128,256]{1,0:T(8,128)(2,1)} async-done(((bf16[1024,256]{1,0:T(8,128)(2,1)}), bf16[128,256]{1,0:T(8,128)(2,1)}) %reduce-scatter.22.cloned.1.call-update) | async-done | bytes 65552
  123.0 14.0 %all_gather.13 = bf16[256,1024]{1,0:T(8,128)(2,1)S(1)} all-gather(bf16[256,128]{1,0:T(8,128)(2,1)S(1)} %add_convert_fusion.2), channel_id=1, replica_groups=mesh['kv'=4,'tp'=8] {'tp'}, dimensions={1}, use_global_device_ids=true | all-gather | bytes 589824 | tf_op jit(solution)/shard_map/all_gather | solution.py:167
  137.1 2.0 convolution_convert_fusion.8
  140.4 2.0 convolution_convert_fusion.7
  142.5 2.4 convolution_convert_fusion.5
  145.1 9.9 %all-reduce = bf16[256]{0:T(256)(128)(2,1)S(1)} all-reduce(bf16[256]{0:T(256)(128)(2,1)S(1)} %fusion.5), channel_id=4, replica_groups=mesh['kv'=4,'tp'=8] {'kv'}, use_global_device_ids=true, to_apply=%region_7.8.clone | all-reduce | flops 256 | bytes 1024
  155.2 2.4 convolution_convert_fusion.6
  157.8 4.2 %reduce-scatter.16.cloned.1.call-done = bf16[64,256]{1,0:T(8,128)(2,1)} async-done(((bf16[256,256]{1,0:T(8,128)(2,1)}), bf16[64,256]{1,0:T(8,128)(2,1)}) %reduce-scatter.16.cloned.1.call-update) | async-done | bytes 32784 | tf_op jit(solution)/shard_map/reduce_scatter | solution.py:69
  162.0 26.8 %reduce-scatter.18.cloned.1.call-done = bf16[64,256]{1,0:T(8,128)(2,1)} async-done(((bf16[256,256]{1,0:T(8,128)(2,1)}), bf16[64,256]{1,0:T(8,128)(2,1)}) %reduce-scatter.18.cloned.1.call-update) | async-done | bytes 32784 | tf_op jit(solution)/shard_map/reduce_scatter | solution.py:72
  190.2 26.1 %reduce-scatter.20.cloned.1.call-done = bf16[64,512]{1,0:T(8,128)(2,1)} async-done(((bf16[256,512]{1,0:T(8,128)(2,1)}), bf16[64,512]{1,0:T(8,128)(2,1)}) %reduce-scatter.20.cloned.1.call-update) | async-done | bytes 65552 | tf_op jit(solution)/shard_map/reduce_scatter | solution.py:75
  217.3 5.3 %multiply_add_fusion = f32[64,4,64,128]{3,2,1,0:T(8,128)S(1)} fusion(f32[64,4,64,128]{3,2,1,0:T(8,128)} %param.18, f32[64,4,128]{2,1,0:T(4,128)S(1)} %mul.290, f32[64,4,64]{2,1,0:T(4,128)S(1)} %copy.21, f32[4]{0:T(128)S(1)} %exponential_subtract_fusion), kind=kLoop, calls=%fused_computation | loop fusion | flops 6291456 | bytes 16973840 | tf_op jit(solution)/shard_map/add | solution.py:97
  222.6 7.3 %fusion.30 = f32[64,4,1,128]{3,2,1,0:T(1,128)S(1)} fusion(f32[64,4,64,1]{2,3,1,0:T(1,128)S(1)} %copy.22, f32[64,4,64,128]{3,2,1,0:T(8,128)S(1)} %multiply_add_fusion), kind=kOutput, calls=%fused_computation.64 | convolution fusion | flops 25165824 | bytes 8585216 | tf_op jit(solution)/shard_map/bhk,bhkv->bhv/dot_general | solution.py:100
  230.6 12.7 %reduce-scatter.14.cloned.1.call-done = bf16[64,512]{1,0:T(8,128)(2,1)} async-done(((bf16[256,512]{1,0:T(8,128)(2,1)}), bf16[64,512]{1,0:T(8,128)(2,1)}) %reduce-scatter.14.cloned.1.call-update) | async-done | bytes 65552 | tf_op jit(solution)/shard_map/reduce_scatter | solution.py:78
  244.3 9.3 %all_gather.14 = bf16[256,512]{1,0:T(8,128)(2,1)S(1)} all-gather(bf16[64,512]{1,0:T(8,128)(2,1)S(1)} %fusion.21), channel_id=1, replica_groups=mesh['kv'=4,'tp'=8] {'kv'}, dimensions={0}, use_global_device_ids=true | all-gather | bytes 327680 | tf_op jit(solution)/shard_map/all_gather | solution.py:108
  253.6 1.7 convolution_convert_fusion.4
  255.2 1.0 copy.26
  256.3 31.4 %reduce-scatter.24.cloned.1.call-done = bf16[128,256]{1,0:T(8,128)(2,1)} async-done(((bf16[1024,256]{1,0:T(8,128)(2,1)}), bf16[128,256]{1,0:T(8,128)(2,1)}) %reduce-scatter.24.cloned.1.call-update) | async-done | bytes 65552
  288.7 14.2 %all_gather.15 = bf16[256,1024]{1,0:T(8,128)(2,1)S(1)} all-gather(bf16[256,128]{1,0:T(8,128)(2,1)S(1)} %add_convert_fusion.1), channel_id=1, replica_groups=mesh['kv'=4,'tp'=8] {'tp'}, dimensions={1}, use_global_device_ids=true | all-gather | bytes 589824 | tf_op jit(solution)/shard_map/all_gather | solution.py:167
  302.8 3.7 convolution_convert_fusion
  306.5 1.9 convolution_convert_fusion.1
  308.6 10.2 %psum.46 = bf16[256]{0:T(256)(128)(2,1)S(1)} all-reduce(bf16[256]{0:T(256)(128)(2,1)S(1)} %fusion.7), channel_id=1, replica_groups=mesh['kv'=4,'tp'=8] {'kv'}, use_global_device_ids=true, to_apply=%region_16.17 | all-reduce | flops 256 | bytes 1024 | tf_op jit(solution)/shard_map/psum | solution.py:43
  318.9 46.7 %all-reduce.6.cloned.1.call-done = (bf16[256,1408]{1,0:T(8,128)(2,1)}, bf16[256,1408]{1,0:T(8,128)(2,1)}) async-done(((bf16[256,1408]{1,0:T(8,128)(2,1)}, bf16[256,1408]{1,0:T(8,128)(2,1)}), (bf16[256,1408]{1,0:T(8,128)(2,1)}, bf16[256,1408]{1,0:T(8,128)(2,1)})) %all-reduce.6.cloned.1.call-update) | async-done | bytes 1441808 | tf_op jit(solution)/shard_map/psum | solution.py:42
  365.6 3.4 fusion.1
  369.0 1.0 copy.28
  370.0 31.6 %reduce-scatter.26.cloned.1.call-done = bf16[128,256]{1,0:T(8,128)(2,1)} async-done(((bf16[1024,256]{1,0:T(8,128)(2,1)}), bf16[128,256]{1,0:T(8,128)(2,1)}) %reduce-scatter.26.cloned.1.call-update) | async-done | bytes 65552
  (69 shorter events, 9.5 us)
Async XLA Ops:
  7.2 15.9 %copy-start = (bf16[1024,1408]{1,0:T(8,128)(2,1)S(1)}, bf16[1024,1408]{1,0:T(8,128)(2,1)}, u32[]{:S(2)}) copy-start(bf16[1024,1408]{1,0:T(8,128)(2,1)} %param.21) | copy-start | bytes 8650756
  7.2 18.4 %copy-start.6 = (f32[1024]{0:T(1024)S(1)}, f32[1024]{0:T(1024)}, u32[]{:S(2)}) copy-start(f32[1024]{0:T(1024)} %param.19) | copy-start | bytes 12292
  7.2 79.0 %all-reduce.8.cloned.1.call-start = ((), (), s32[]{:S(2)}) async-start(), calls=%async_computation.15 | async-start | bytes 2883584 | tf_op jit(solution)/shard_map/psum | solution.py:42
  7.2 18.3 %copy-start.4 = (bf16[1024,1408]{1,0:T(8,128)(2,1)S(1)}, bf16[1024,1408]{1,0:T(8,128)(2,1)}, u32[]{:S(2)}) copy-start(bf16[1024,1408]{1,0:T(8,128)(2,1)} %param.20) | copy-start | bytes 8650756
  27.5 94.6 %reduce-scatter.22.cloned.1.call-start = ((), (), s32[]{:S(2)}) async-start(), calls=%async_computation.11 | async-start | bytes 589824
  86.2 36.8 %copy-start.2 = (bf16[256,128]{1,0:T(8,128)(2,1)S(1)}, bf16[256,128]{1,0:T(8,128)(2,1)}, u32[]{:S(2)}) copy-start(bf16[256,128]{1,0:T(8,128)(2,1)} %param.17) | copy-start | bytes 196612
  86.2 50.9 %copy-start.7 = (f32[1024]{0:T(1024)S(1)}, f32[1024]{0:T(1024)}, u32[]{:S(2)}) copy-start(f32[1024]{0:T(1024)} %param.23) | copy-start | bytes 12292
  89.7 49.5 %copy-start.9 = (u32[32]{0:T(128)S(1)}, u32[32]{0:T(128)}, u32[]{:S(2)}) copy-start(u32[32]{0:T(128)} %constant.53) | copy-start | bytes 388
  90.7 71.3 %reduce-scatter.16.cloned.1.call-start = ((), (), s32[]{:S(2)}) async-start(), calls=%async_computation.8 | async-start | bytes 163840 | tf_op jit(solution)/shard_map/reduce_scatter | solution.py:69
  139.1 49.7 %reduce-scatter.18.cloned.1.call-start = ((), (), s32[]{:S(2)}) async-start(), calls=%async_computation.9 | async-start | bytes 163840 | tf_op jit(solution)/shard_map/reduce_scatter | solution.py:72
  142.4 73.9 %reduce-scatter.20.cloned.1.call-start = ((), (), s32[]{:S(2)}) async-start(), calls=%async_computation.10 | async-start | bytes 327680 | tf_op jit(solution)/shard_map/reduce_scatter | solution.py:75
  144.9 98.4 %reduce-scatter.14.cloned.1.call-start = ((), (), s32[]{:S(2)}) async-start(), calls=%async_computation.7 | async-start | bytes 327680 | tf_op jit(solution)/shard_map/reduce_scatter | solution.py:78
  157.6 130.1 %reduce-scatter.24.cloned.1.call-start = ((), (), s32[]{:S(2)}) async-start(), calls=%async_computation.12 | async-start | bytes 589824
  222.6 7.4 %copy-start.1 = (f32[64,4,64,128]{3,2,1,0:T(8,128)}, f32[64,4,64,128]{3,2,1,0:T(8,128)S(1)}, u32[]{:S(2)}) copy-start(f32[64,4,64,128]{3,2,1,0:T(8,128)S(1)} %multiply_add_fusion) | copy-start | bytes 25165828
  222.6 20.7 %copy-start.3 = (f32[512]{0:T(512)S(1)}, f32[512]{0:T(512)}, u32[]{:S(2)}) copy-start(f32[512]{0:T(512)} %param.28) | copy-start | bytes 6148
  230.0 72.8 %copy-start.8 = (f32[1024]{0:T(1024)S(1)}, f32[1024]{0:T(1024)}, u32[]{:S(2)}) copy-start(f32[1024]{0:T(1024)} %param.30) | copy-start | bytes 12292
  256.2 109.3 %all-reduce.6.cloned.1.call-start = ((), (), s32[]{:S(2)}) async-start(), calls=%async_computation.14 | async-start | bytes 2883584 | tf_op jit(solution)/shard_map/psum | solution.py:42
  288.6 17.9 %copy-start.5 = (bf16[1024,1408]{1,0:T(8,128)(2,1)S(1)}, bf16[1024,1408]{1,0:T(8,128)(2,1)}, u32[]{:S(2)}) copy-start(bf16[1024,1408]{1,0:T(8,128)(2,1)} %param.31) | copy-start | bytes 8650756
  308.4 93.2 %reduce-scatter.26.cloned.1.call-start = ((), (), s32[]{:S(2)}) async-start(), calls=%async_computation.13 | async-start | bytes 589824
Sparse Core Ops, SparseCore 0:
  27.6 58.5 all-reduce.7
  90.8 31.1 reduce-scatter.21
  139.2 22.7 reduce-scatter.15
  164.6 24.1 reduce-scatter.17
  192.0 24.3 reduce-scatter.19
  218.9 24.3 reduce-scatter.13
  256.4 31.2 reduce-scatter.23
  308.5 56.9 all-reduce.5
  370.1 31.3 reduce-scatter.25
where the time goes:
time: 411 us; the launch traced here: 410 us
  waiting for transfers between devices  259 us (63%)
  blocking collectives  83.5 us (20%)
  matrix products  34.6 us (8%)
  between operations  14.8 us (4%)
  other arithmetic  10.2 us (2%)
  local copies, waits for them, and re-layouts  6.92 us (2%)
    psum x2, waiting for transfers between devices, channel_mix(): lax.psum(up_part.astype(jnp.bfloat16), 'kv').astype(jnp.float32)  95.1 us
    unnamed x12, waiting for transfers between devices  94.3 us
    all_gather x2, blocking collectives, shards(): widened = lax.all_gather(own_columns, 'tp', axis=1, tiled=True)  28.2 us
    reduce_scatter x1, waiting for transfers between devices, token_mix(): lax.psum_scatter(key_part.astype(jnp.bfloat16), 'kv', scatter_dimension=0...  26.8 us
    reduce_scatter x1, waiting for transfers between devices, token_mix(): lax.psum_scatter(value_part.astype(jnp.bfloat16), 'kv', scatter_dimension...  26.1 us
    psum x2, blocking collectives, channel_mix(): lax.psum(squares.astype(jnp.bfloat16), 'kv').astype(jnp.float32)  20.3 us
    all_gather x1, blocking collectives, shards(): widened = lax.all_gather(tokens, 'tp', axis=1, tiled=True)  15.8 us
    reduce_scatter x1, waiting for transfers between devices, token_mix(): lax.psum_scatter(gate_part.astype(jnp.bfloat16), 'kv', scatter_dimension=...  12.7 us
  transfers between devices with their start and end apart: 9, of which 9 were waited for; matrix products, arithmetic and copies ran while one was open for 6% of the time, Pallas kernels for 0%

commit v1 on v0

--- a/solution.py
+++ b/solution.py
@@ -164,7 +164,8 @@
         ).astype(jnp.float32)
         own_columns = (own_columns.astype(jnp.float32) + own_piece).astype(jnp.bfloat16)
         if section_index < 2:
-            widened = lax.all_gather(own_columns, "tp", axis=1, tiled=True)
+            next_value = jax.lax.all_gather(own_columns, "tp")
+            widened = jnp.concatenate(next_value, axis=1)
     return (own_columns, state_out)
 
 

time: 411 us -> 422 us (1.027)
  local copies, waits for them, and re-layouts: 6.92 us -> 12.9 us
  other arithmetic: 10.2 us -> 15.3 us
    reduce_scatter x1, waiting for transfers between devices: 26.8 us -> 3.41 us  [token_mix(): lax.psum_scatter(key_part.astype(jnp.bfloat16), 'kv', scatter_dimension=0...]
    reduce_scatter x1, waiting for transfers between devices: 4.2 us -> 26.8 us  [token_mix(): lax.psum_scatter(query_part.astype(jnp.bfloat16), 'kv', scatter_dimension...]
    convert_element_type x0 -> x2, local copies, waits for them, and re-layouts: none -> 5.16 us  [the longest x1 2.59 us: channel_mix(): widened_f = widened.astype(jnp.float32)]
    convert_element_type x0 -> x4, other arithmetic: none -> 5.1 us  [the longest x1 1.57 us: channel_mix(): scaled = (widened_f * gain).astype(jnp.bfloat16)]
where the time goes in v1:
time: 422 us
  waiting for transfers between devices  258 us (61%)
  blocking collectives  84.9 us (20%)
  matrix products  35.2 us (8%)
  other arithmetic  15.3 us (4%)
  between operations  14.8 us (4%)
  local copies, waits for them, and re-layouts  12.9 us (3%)
    psum x2, waiting for transfers between devices, channel_mix(): lax.psum(up_part.astype(jnp.bfloat16), 'kv').astype(jnp.float32)  94.9 us
    unnamed x12, waiting for transfers between devices  94.5 us
    all_gather x2, blocking collectives, shards(): next_value = jax.lax.all_gather(own_columns, 'tp')  30.1 us
    reduce_scatter x1, waiting for transfers between devices, token_mix(): lax.psum_scatter(query_part.astype(jnp.bfloat16), 'kv', scatter_dimension...  26.8 us
    reduce_scatter x1, waiting for transfers between devices, token_mix(): lax.psum_scatter(value_part.astype(jnp.bfloat16), 'kv', scatter_dimension...  25.6 us
    psum x2, blocking collectives, channel_mix(): lax.psum(squares.astype(jnp.bfloat16), 'kv').astype(jnp.float32)  20.1 us
    all_gather x1, blocking collectives, shards(): widened = lax.all_gather(tokens, 'tp', axis=1, tiled=True)  15.8 us
    reduce_scatter x1, waiting for transfers between devices, token_mix(): lax.psum_scatter(gate_part.astype(jnp.bfloat16), 'kv', scatter_dimension=...  12.7 us
  transfers between devices with their start and end apart: 9, of which 9 were waited for; matrix products, arithmetic and copies ran while one was open for 6% of the time, Pallas kernels for 0%

profile of v1, /device:TPU:0, one launch (start us, length us, event | category | flops | bytes accessed | tf_op | source)
XLA Modules:
  0.0 421.6 jit_solution(11288777733232759057)
XLA Ops:
  7.2 15.8 %all_gather.18 = bf16[256,1024]{1,0:T(8,128)(2,1)S(1)} all-gather(bf16[256,128]{1,0:T(8,128)(2,1)} %param.17), channel_id=1, replica_groups=mesh['kv'=4,'tp'=8] {'tp'}, dimensions={1}, use_global_device_ids=true | all-gather | bytes 589824 | tf_op jit(solution)/shard_map/all_gather | solution.py:156
  23.0 2.5 convolution_convert_fusion.2
  25.6 1.9 convolution_convert_fusion.3
  27.7 10.1 %psum.43 = bf16[256]{0:T(256)(128)(2,1)S(1)} all-reduce(bf16[256]{0:T(256)(128)(2,1)S(1)} %fusion.3), channel_id=1, replica_groups=mesh['kv'=4,'tp'=8] {'kv'}, use_global_device_ids=true, to_apply=%region_2.0 | all-reduce | flops 256 | bytes 1024 | tf_op jit(solution)/shard_map/psum | solution.py:43
  37.8 48.4 %all-reduce.8.cloned.1.call-done = (bf16[256,1408]{1,0:T(8,128)(2,1)}, bf16[256,1408]{1,0:T(8,128)(2,1)}) async-done(((bf16[256,1408]{1,0:T(8,128)(2,1)}, bf16[256,1408]{1,0:T(8,128)(2,1)}), (bf16[256,1408]{1,0:T(8,128)(2,1)}, bf16[256,1408]{1,0:T(8,128)(2,1)})) %all-reduce.8.cloned.1.call-update) | async-done | bytes 1441808 | tf_op jit(solution)/shard_map/psum | solution.py:42
  86.2 3.5 fusion
  90.8 31.5 %reduce-scatter.22.cloned.1.call-done = bf16[128,256]{1,0:T(8,128)(2,1)} async-done(((bf16[1024,256]{1,0:T(8,128)(2,1)}), bf16[128,256]{1,0:T(8,128)(2,1)}) %reduce-scatter.22.cloned.1.call-update) | async-done | bytes 65552
  123.3 14.9 %all-gather = bf16[2048,128]{1,0:T(8,128)(2,1)S(1)} all-gather(bf16[256,128]{1,0:T(8,128)(2,1)S(1)} %add_convert_fusion.2), channel_id=2, replica_groups=mesh['kv'=4,'tp'=8] {'tp'}, dimensions={0}, use_global_device_ids=true | all-gather | bytes 589824 | tf_op jit(solution)/shard_map/all_gather | solution.py:167
  139.2 2.6 copy.23
  144.0 2.0 convolution_convert_fusion.7
  147.4 2.2 convolution_convert_fusion.8
  149.7 2.6 convolution_convert_fusion.5
  152.5 9.7 %all-reduce = bf16[256]{0:T(256)(128)(2,1)S(1)} all-reduce(bf16[256]{0:T(256)(128)(2,1)S(1)} %fusion.4), channel_id=6, replica_groups=mesh['kv'=4,'tp'=8] {'kv'}, use_global_device_ids=true, to_apply=%region_7.8.clone | all-reduce | flops 256 | bytes 1024
  162.2 2.6 convolution_convert_fusion.6
  165.1 3.4 reduce-scatter.18.cloned.1.call-done
  168.5 26.8 %reduce-scatter.16.cloned.1.call-done = bf16[64,256]{1,0:T(8,128)(2,1)} async-done(((bf16[256,256]{1,0:T(8,128)(2,1)}), bf16[64,256]{1,0:T(8,128)(2,1)}) %reduce-scatter.16.cloned.1.call-update) | async-done | bytes 32784 | tf_op jit(solution)/shard_map/reduce_scatter | solution.py:69
  196.7 25.6 %reduce-scatter.20.cloned.1.call-done = bf16[64,512]{1,0:T(8,128)(2,1)} async-done(((bf16[256,512]{1,0:T(8,128)(2,1)}), bf16[64,512]{1,0:T(8,128)(2,1)}) %reduce-scatter.20.cloned.1.call-update) | async-done | bytes 65552 | tf_op jit(solution)/shard_map/reduce_scatter | solution.py:75
  223.2 5.3 %multiply_add_fusion = f32[64,4,64,128]{3,2,1,0:T(8,128)S(1)} fusion(f32[64,4,64,128]{3,2,1,0:T(8,128)} %param.18, f32[64,4,128]{2,1,0:T(4,128)S(1)} %mul.294, f32[64,4,64]{2,1,0:T(4,128)S(1)} %copy.26, f32[4]{0:T(128)S(1)} %exponential_subtract_fusion), kind=kLoop, calls=%fused_computation | loop fusion | flops 6291456 | bytes 16973840 | tf_op jit(solution)/shard_map/add | solution.py:97
  228.6 7.3 %fusion.24 = f32[64,4,1,128]{3,2,1,0:T(1,128)S(1)} fusion(f32[64,4,64,1]{2,3,1,0:T(1,128)S(1)} %copy.28, f32[64,4,64,128]{3,2,1,0:T(8,128)S(1)} %multiply_add_fusion), kind=kOutput, calls=%fused_computation.66 | convolution fusion | flops 25165824 | bytes 8585216 | tf_op jit(solution)/shard_map/bhk,bhkv->bhv/dot_general | solution.py:100
  236.5 12.7 %reduce-scatter.14.cloned.1.call-done = bf16[64,512]{1,0:T(8,128)(2,1)} async-done(((bf16[256,512]{1,0:T(8,128)(2,1)}), bf16[64,512]{1,0:T(8,128)(2,1)}) %reduce-scatter.14.cloned.1.call-update) | async-done | bytes 65552 | tf_op jit(solution)/shard_map/reduce_scatter | solution.py:78
  250.2 9.3 %all_gather.21 = bf16[256,512]{1,0:T(8,128)(2,1)S(1)} all-gather(bf16[64,512]{1,0:T(8,128)(2,1)S(1)} %fusion.15), channel_id=1, replica_groups=mesh['kv'=4,'tp'=8] {'kv'}, dimensions={0}, use_global_device_ids=true | all-gather | bytes 327680 | tf_op jit(solution)/shard_map/all_gather | solution.py:108
  259.5 1.7 convolution_convert_fusion.4
  262.2 31.5 %reduce-scatter.24.cloned.1.call-done = bf16[128,256]{1,0:T(8,128)(2,1)} async-done(((bf16[1024,256]{1,0:T(8,128)(2,1)}), bf16[128,256]{1,0:T(8,128)(2,1)}) %reduce-scatter.24.cloned.1.call-update) | async-done | bytes 65552
  294.7 15.2 %all-gather.1 = bf16[2048,128]{1,0:T(8,128)(2,1)S(1)} all-gather(bf16[256,128]{1,0:T(8,128)(2,1)S(1)} %add_convert_fusion.1), channel_id=3, replica_groups=mesh['kv'=4,'tp'=8] {'tp'}, dimensions={0}, use_global_device_ids=true | all-gather | bytes 589824 | tf_op jit(solution)/shard_map/all_gather | solution.py:167
  310.9 2.6 copy.27
  313.5 1.6 fusion.6
  315.1 3.7 convolution_convert_fusion
  318.8 1.9 convolution_convert_fusion.1
  321.0 10.0 %psum.46 = bf16[256]{0:T(256)(128)(2,1)S(1)} all-reduce(bf16[256]{0:T(256)(128)(2,1)S(1)} %fusion.5), channel_id=1, replica_groups=mesh['kv'=4,'tp'=8] {'kv'}, use_global_device_ids=true, to_apply=%region_16.17 | all-reduce | flops 256 | bytes 1024 | tf_op jit(solution)/shard_map/psum | solution.py:43
  331.0 46.5 %all-reduce.6.cloned.1.call-done = (bf16[256,1408]{1,0:T(8,128)(2,1)}, bf16[256,1408]{1,0:T(8,128)(2,1)}) async-done(((bf16[256,1408]{1,0:T(8,128)(2,1)}, bf16[256,1408]{1,0:T(8,128)(2,1)}), (bf16[256,1408]{1,0:T(8,128)(2,1)}, bf16[256,1408]{1,0:T(8,128)(2,1)})) %all-reduce.6.cloned.1.call-update) | async-done | bytes 1441808 | tf_op jit(solution)/shard_map/psum | solution.py:42
  377.5 3.4 fusion.1
  382.0 31.5 %reduce-scatter.26.cloned.1.call-done = bf16[128,256]{1,0:T(8,128)(2,1)} async-done(((bf16[1024,256]{1,0:T(8,128)(2,1)}), bf16[128,256]{1,0:T(8,128)(2,1)}) %reduce-scatter.26.cloned.1.call-update) | async-done | bytes 65552
  (77 shorter events, 16.8 us)
Async XLA Ops:
  7.2 15.9 %copy-start = (bf16[1024,1408]{1,0:T(8,128)(2,1)S(1)}, bf16[1024,1408]{1,0:T(8,128)(2,1)}, u32[]{:S(2)}) copy-start(bf16[1024,1408]{1,0:T(8,128)(2,1)} %param.21) | copy-start | bytes 8650756
  7.2 18.4 %copy-start.9 = (f32[1024]{0:T(1024)S(1)}, f32[1024]{0:T(1024)}, u32[]{:S(2)}) copy-start(f32[1024]{0:T(1024)} %param.19) | copy-start | bytes 12292
  7.2 79.0 %all-reduce.8.cloned.1.call-start = ((), (), s32[]{:S(2)}) async-start(), calls=%async_computation.15 | async-start | bytes 2883584 | tf_op jit(solution)/shard_map/psum | solution.py:42
  7.2 18.3 %copy-start.7 = (bf16[1024,1408]{1,0:T(8,128)(2,1)S(1)}, bf16[1024,1408]{1,0:T(8,128)(2,1)}, u32[]{:S(2)}) copy-start(bf16[1024,1408]{1,0:T(8,128)(2,1)} %param.20) | copy-start | bytes 8650756
  27.5 94.8 %reduce-scatter.22.cloned.1.call-start = ((), (), s32[]{:S(2)}) async-start(), calls=%async_computation.11 | async-start | bytes 589824
  86.2 37.0 %copy-start.3 = (bf16[256,128]{1,0:T(8,128)(2,1)S(1)}, bf16[256,128]{1,0:T(8,128)(2,1)}, u32[]{:S(2)}) copy-start(bf16[256,128]{1,0:T(8,128)(2,1)} %param.17) | copy-start | bytes 196612
  89.7 52.2 %copy-start.4 = (f32[1024]{0:T(1024)S(1)}, f32[1024]{0:T(1024)}, u32[]{:S(2)}) copy-start(f32[1024]{0:T(1024)} %param.23) | copy-start | bytes 12292
  90.7 77.8 %reduce-scatter.18.cloned.1.call-start = ((), (), s32[]{:S(2)}) async-start(), calls=%async_computation.9 | async-start | bytes 163840 | tf_op jit(solution)/shard_map/reduce_scatter | solution.py:72
  139.2 6.9 %copy-start.10 = (u32[32]{0:T(128)S(1)}, u32[32]{0:T(128)}, u32[]{:S(2)}) copy-start(u32[32]{0:T(128)} %constant.53) | copy-start | bytes 388
  143.2 0.8 copy-start.2
  146.1 49.2 %reduce-scatter.16.cloned.1.call-start = ((), (), s32[]{:S(2)}) async-start(), calls=%async_computation.8 | async-start | bytes 163840 | tf_op jit(solution)/shard_map/reduce_scatter | solution.py:69
  149.6 72.6 %reduce-scatter.20.cloned.1.call-start = ((), (), s32[]{:S(2)}) async-start(), calls=%async_computation.10 | async-start | bytes 327680 | tf_op jit(solution)/shard_map/reduce_scatter | solution.py:75
  152.3 97.0 %reduce-scatter.14.cloned.1.call-start = ((), (), s32[]{:S(2)}) async-start(), calls=%async_computation.7 | async-start | bytes 327680 | tf_op jit(solution)/shard_map/reduce_scatter | solution.py:78
  164.8 128.9 %reduce-scatter.24.cloned.1.call-start = ((), (), s32[]{:S(2)}) async-start(), calls=%async_computation.12 | async-start | bytes 589824
  228.5 7.4 %copy-start.1 = (f32[64,4,64,128]{3,2,1,0:T(8,128)}, f32[64,4,64,128]{3,2,1,0:T(8,128)S(1)}, u32[]{:S(2)}) copy-start(f32[64,4,64,128]{3,2,1,0:T(8,128)S(1)} %multiply_add_fusion) | copy-start | bytes 25165828
  228.6 20.7 %copy-start.6 = (f32[512]{0:T(512)S(1)}, f32[512]{0:T(512)}, u32[]{:S(2)}) copy-start(f32[512]{0:T(512)} %param.28) | copy-start | bytes 6148
  261.1 52.4 %copy-start.5 = (f32[1024]{0:T(1024)S(1)}, f32[1024]{0:T(1024)}, u32[]{:S(2)}) copy-start(f32[1024]{0:T(1024)} %param.30) | copy-start | bytes 12292
  262.2 115.3 %all-reduce.6.cloned.1.call-start = ((), (), s32[]{:S(2)}) async-start(), calls=%async_computation.14 | async-start | bytes 2883584 | tf_op jit(solution)/shard_map/psum | solution.py:42
  313.5 5.3 %copy-start.8 = (bf16[1024,1408]{1,0:T(8,128)(2,1)S(1)}, bf16[1024,1408]{1,0:T(8,128)(2,1)}, u32[]{:S(2)}) copy-start(bf16[1024,1408]{1,0:T(8,128)(2,1)} %param.31) | copy-start | bytes 8650756
  320.7 92.7 %reduce-scatter.26.cloned.1.call-start = ((), (), s32[]{:S(2)}) async-start(), calls=%async_computation.13 | async-start | bytes 589824
Sparse Core Ops, SparseCore 0:
  27.6 58.5 all-reduce.7
  90.8 31.3 reduce-scatter.21
  146.2 22.1 reduce-scatter.17
  171.1 24.1 reduce-scatter.15
  197.9 24.3 reduce-scatter.19
  224.9 24.3 reduce-scatter.13
  262.3 31.3 reduce-scatter.23
  320.8 56.5 all-reduce.5
  382.1 31.2 reduce-scatter.25
